TPU v7x, 32 devices: a whole 2x2x4 slice. The times are simulated.
32 devices in a mesh: grp: 2 (over y), sp: 4 (over z), tp: 4 (over x, core).
Axes of the slice: x: 2, y: 2, z: 4, core: 2. Of those that a mesh axis runs over, the one named last changes fastest.
Arguments:
- tokens: bfloat16 [2048, 2048], P(('grp', 'sp'), 'tp'), parts along dimension 0, may hold values from -40 to 40
- norm_gain: float32 [2, 2048], replicated, may hold values from 0.1 to 1.9
- value_proj: bfloat16 [2, 1024, 2048], P(None, 'tp', 'sp'), may hold values from -0.125 to 0.125
- gate_proj: bfloat16 [2, 1024, 2048], P(None, 'tp', 'sp'), may hold values from -0.125 to 0.125
- conv_taps: float32 [2, 4, 1024], P(None, None, 'tp'), may hold values from -3 to 3
- recur_map: bfloat16 [2, 16, 64, 64], P(None, 'tp'), may hold values from -0.75 to 0.75
- input_map: bfloat16 [2, 16, 64, 64], P(None, 'tp'), may hold values from -0.75 to 0.75
- decay_param: float32 [2, 1024], P(None, 'tp'), may hold values from 3 to 16
- decay_offset: float32 [2, 1024, 1024], P(None, 'tp', 'sp'), may hold values from -3 to 0
- mix_proj: bfloat16 [2, 1024, 2048], P(None, 'sp', 'tp'), may hold values from -0.1875 to 0.1875
Outputs:
- mixed_out: bfloat16 [2048, 2048], P(('grp', 'sp'), 'tp'), parts along dimension 0
There are 2 independent parts, one for each index of `grp`. A program takes and returns all parts, laid end to end along the dimension named above; an argument that names none is the same for every part. Nothing has to cross between parts.
All inputs are finite; a program needn't handle non-finite values.
Results may differ from a plain program's by a relative error of at most 0.013.
Values may be sent and summed in bfloat16 or wider, within the bound.
A program may use at most 64 MiB of HBM per device.

v0:
```python
import jax
import jax.numpy as jnp
from jax import lax
from jax.sharding import PartitionSpec as P

LAYERS = 2


EPS = 1e-06
RATE_SCALE = 8.0


def from_behind(value, axis, steps):
    count = lax.axis_size(axis)
    first, last = (max(0, -steps), min(count, count - steps))
    return lax.ppermute(value, axis, [(source, source + steps) for source in range(first, last)])


def carried_in(value, axis, join, neutral):
    count, mine = (lax.axis_size(axis), lax.axis_index(axis))
    pieces = jax.tree.map(lambda part: lax.all_gather(part, axis), value)
    total = jax.tree.map(
        lambda part, zero: jnp.full_like(part, 0) + jnp.asarray(zero, part.dtype), value, neutral
    )

    def step(position, total):
        longer = join(total, jax.tree.map(lambda part: part[position], pieces))
        return jax.tree.map(lambda new, old: jnp.where(position < mine, new, old), longer, total)

    return lax.fori_loop(0, count - 1, step, total)


def combine_pairs(earlier, later):
    return (earlier[0] * later[0], later[0] * earlier[1] + later[1])


def local(
    tokens,
    norm_gain,
    value_proj,
    gate_proj,
    conv_taps,
    recur_map,
    input_map,
    decay_param,
    decay_offset,
    mix_proj,
):
    tok_rows = tokens.shape[0]
    own_cols = tokens.shape[1]
    channels = value_proj.shape[1]
    heads_here = recur_map.shape[1]
    head_size = recur_map.shape[2]
    filter_tap_total = conv_taps.shape[1]
    full_width = own_cols * lax.axis_size("tp")
    col_start = lax.axis_index("tp") * own_cols
    every_value, every_gate, every_mix = (
        lax.all_gather(value_proj, "sp", axis=2, tiled=True),
        lax.all_gather(gate_proj, "sp", axis=2, tiled=True),
        lax.all_gather(mix_proj, "sp", axis=1, tiled=True),
    )
    residual = tokens
    for layer_index in range(LAYERS):
        value_weights = every_value[layer_index]
        gate_weights = every_gate[layer_index]
        mix_weights = every_mix[layer_index]
        both_weights = jnp.concatenate([value_weights, gate_weights], axis=0)
        gain_row = norm_gain[layer_index]
        wide = residual.astype(jnp.float32)
        squares = lax.psum(jnp.sum(wide * wide, axis=1), "tp")
        own_gain = lax.dynamic_slice_in_dim(gain_row, col_start, own_cols)
        scaled = (wide * own_gain[None, :]).astype(jnp.bfloat16)
        unscaled = lax.dot_general(
            both_weights,
            lax.all_gather(scaled, "tp", axis=1, tiled=True),
            (((1,), (1,)), ((), ())),
            preferred_element_type=jnp.float32,
        )
        scale_factor = lax.rsqrt(squares / full_width + EPS)
        projected = unscaled * scale_factor[None, :]
        value_rows = projected[:channels].astype(jnp.bfloat16)
        gate_rows = projected[channels:].astype(jnp.bfloat16)
        before = from_behind(value_rows[:, tok_rows - (filter_tap_total - 1) :], "sp", 1)
        padded = jnp.concatenate([before, value_rows], axis=1)
        taps_layer = conv_taps[layer_index]
        smoothed = jnp.zeros((channels, tok_rows), jnp.float32)
        for tap_index in range(filter_tap_total):
            smoothed = smoothed + taps_layer[tap_index][:, None] * padded[
                :, tap_index : tap_index + tok_rows
            ].astype(jnp.float32)
        smoothed_half = smoothed.astype(jnp.bfloat16).reshape(heads_here, head_size, tok_rows)
        recur = jax.nn.sigmoid(
            jnp.einsum(
                "hit,hij->hjt",
                smoothed_half,
                recur_map[layer_index],
                preferred_element_type=jnp.float32,
            ).reshape(channels, tok_rows)
        )
        inputs = jax.nn.sigmoid(
            jnp.einsum(
                "hit,hij->hjt",
                smoothed_half,
                input_map[layer_index],
                preferred_element_type=jnp.float32,
            ).reshape(channels, tok_rows)
        )
        log_decay = (
            -RATE_SCALE * recur * jax.nn.softplus(-decay_param[layer_index])[:, None]
            + decay_offset[layer_index]
        )
        decay = jnp.exp(log_decay)
        driving = jnp.sqrt(-jnp.expm1(2.0 * log_decay)) * inputs * smoothed
        cumulative, local_state = lax.associative_scan(combine_pairs, (decay, driving), axis=1)
        identity = (jnp.ones((channels,), jnp.float32), jnp.zeros((channels,), jnp.float32))
        carried = carried_in((cumulative[:, -1], local_state[:, -1]), "sp", combine_pairs, identity)
        hidden_state = local_state + cumulative * carried[1][:, None]
        branch = (hidden_state * jax.nn.silu(gate_rows.astype(jnp.float32))).astype(jnp.bfloat16)
        mixed_sum = lax.dot_general(
            lax.all_gather(branch, "tp", axis=0, tiled=True),
            mix_weights,
            (((0,), (0,)), ((), ())),
            preferred_element_type=jnp.float32,
        )
        residual = (wide + mixed_sum).astype(jnp.bfloat16)
    return residual


def solution(mesh):
    in_specs = (
        P(("grp", "sp"), "tp"),
        P(),
        P(None, "tp", "sp"),
        P(None, "tp", "sp"),
        P(None, None, "tp"),
        P(None, "tp", None, None),
        P(None, "tp", None, None),
        P(None, "tp"),
        P(None, "tp", "sp"),
        P(None, "sp", "tp"),
    )
    out_specs = P(("grp", "sp"), "tp")
    return jax.shard_map(local, mesh=mesh, in_specs=in_specs, out_specs=out_specs, check_vma=False)
```

profile of v0, /device:TPU:27, one launch (start us, length us, event | category | flops | bytes accessed | tf_op | source)
XLA Modules:
  0.0 230.8 jit_solution(7412309215004755301)
XLA Ops:
  6.5 0.7 all-gather.12.cloned.1.call-update
  7.3 0.7 all-gather.10.cloned.1.call-update
  8.1 0.8 fusion.88
  8.9 1.7 fusion.36
  10.7 0.5 all-gather.16.cloned.1.call-update
  11.3 5.7 %psum.14 = f32[256]{0:T(256)S(1)} all-reduce(f32[256]{0:T(256)S(1)} %get-tuple-element.271), channel_id=1, replica_groups=mesh['grp'=2,'sp'=4,'tp'=4] {'tp'}, use_global_device_ids=true, to_apply=%region_1.0 | all-reduce | flops 256 | bytes 2048 | tf_op jit(solution)/shard_map/psum | solution.py:70
  17.1 36.4 %all-gather.12.cloned.1.call-done = bf16[2,256,2048]{2,1,0:T(8,128)(2,1)} async-done(((bf16[2,256,512]{2,1,0:T(8,128)(2,1)}), bf16[2,256,2048]{2,1,0:T(8,128)(2,1)}) %all-gather.12.cloned.1.call-update) | async-done | bytes 2097168 | tf_op jit(solution)/shard_map/all_gather | solution.py:59
  53.5 1.7 slice_bitcast_fusion.2
  55.2 44.4 %all-gather.10.cloned.1.call-done = bf16[2,256,2048]{2,1,0:T(8,128)(2,1)} async-done(((bf16[2,256,512]{2,1,0:T(8,128)(2,1)}), bf16[2,256,2048]{2,1,0:T(8,128)(2,1)}) %all-gather.10.cloned.1.call-update) | async-done | bytes 2097168 | tf_op jit(solution)/shard_map/all_gather | solution.py:58
  99.6 3.2 %slice_bitcast_fusion.3 = (bf16[256,2048]{1,0:T(8,128)(2,1)}, bf16[256,2048]{1,0:T(8,128)(2,1)}) fusion(bf16[2,256,2048]{2,1,0:T(8,128)(2,1)} %all-gather.10.cloned.1.call-done), kind=kLoop, calls=%fused_computation.41 | loop fusion | bytes 4194304 | tf_op jit(solution)/shard_map/squeeze | solution.py:64
  102.7 15.5 %all-gather.14.cloned.1.call-done = bf16[256,2048]{1,0:T(8,128)(2,1)} async-done(((bf16[256,512]{1,0:T(8,128)(2,1)}), bf16[256,2048]{1,0:T(8,128)(2,1)}) %all-gather.14.cloned.1.call-update) | async-done | bytes 1048592 | tf_op jit(solution)/shard_map/all_gather | solution.py:75
  118.2 2.3 %fusion.17 = bf16[512,256]{0,1:T(8,128)(2,1)S(1)} fusion(bf16[256,2048]{1,0:T(8,128)(2,1)} %all-gather.14.cloned.1.call-done, bf16[256,2048]{1,0:T(8,128)(2,1)S(1)} %get-tuple-element.262, bf16[256,2048]{1,0:T(8,128)(2,1)} %get-tuple-element.260, f32[256]{0:T(256)S(1)} %add_rsqrt_fusion.1), kind=kOutput, calls=%fused_computation.21 | convolution fusion | flops 541327360 | bytes 3408896 | tf_op jit(solution)/shard_map/dot_general | solution.py:73
  120.5 1.4 collective-permute-start
  122.0 0.1 copy.38
  122.2 2.8 %collective-permute-done = bf16[256,3]{0,1:T(4,128)(2,1)S(1)} collective-permute-done((bf16[256,3]{0,1:T(4,128)(2,1)S(1)}, bf16[256,3]{0,1:T(4,128)(2,1)S(1)}, u32[]{:S(2)}, u32[]{:S(2)}) %collective-permute-start) | collective-permute-done | bytes 1568 | tf_op jit(solution)/shard_map/ppermute | solution.py:16
  125.0 0.1 fusion.86
  125.3 0.3 fusion.31
  125.7 0.3 fusion.34
  126.1 0.2 multiply_multiply_fusion.1
  128.2 0.2 slice.678
  128.4 0.2 slice.621
  129.5 6.3 %all-gather = f32[1024,1]{0,1:T(1,128)S(1)} all-gather(f32[256,1]{0,1:T(1,128)S(1)} %slice_add_fusion.5), channel_id=2, replica_groups=mesh['grp'=2,'sp'=4,'tp'=4] {'sp'}, dimensions={0}, use_global_device_ids=true | all-gather | bytes 5120 | tf_op jit(solution)/shard_map/all_gather | solution.py:21
  135.8 0.6 broadcast.232
  136.3 0.6 reduce.12
  137.0 8.1 %all-gather.1 = f32[1024,1]{0,1:T(1,128)S(1)} all-gather(f32[256,1]{0,1:T(1,128)S(1)} %slice_add_fusion.4), channel_id=3, replica_groups=mesh['grp'=2,'sp'=4,'tp'=4] {'sp'}, dimensions={0}, use_global_device_ids=true | all-gather | bytes 5120 | tf_op jit(solution)/shard_map/all_gather | solution.py:21
  145.1 0.6 reduce.13
  145.8 0.2 while.28
  146.1 12.1 %all_gather.38 = bf16[1024,256]{0,1:T(8,128)(2,1)S(1)} all-gather(bf16[256,256]{0,1:T(8,128)(2,1)S(1)} %fusion.46), channel_id=1, replica_groups=mesh['grp'=2,'sp'=4,'tp'=4] {'tp'}, dimensions={0}, use_global_device_ids=true | all-gather | bytes 655360 | tf_op jit(solution)/shard_map/all_gather | solution.py:120
  158.2 5.7 %all-gather.16.cloned.1.call-done = bf16[2,1024,512]{2,1,0:T(8,128)(2,1)} async-done(((bf16[2,256,512]{2,1,0:T(8,128)(2,1)}), bf16[2,1024,512]{2,1,0:T(8,128)(2,1)}) %all-gather.16.cloned.1.call-update) | async-done | bytes 2097168 | tf_op jit(solution)/shard_map/all_gather | solution.py:60
  163.9 2.6 %multiply_reduce_fusion = (f32[256]{0:T(256)S(1)}, bf16[256,512]{1,0:T(8,128)(2,1)}, f32[256,512]{1,0:T(8,128)}) fusion(f32[512]{0:T(512)S(1)} %bitcast.117, bf16[1024,256]{0,1:T(8,128)(2,1)S(1)} %all_gather.38, bf16[2,1024,512]{2,1,0:T(8,128)(2,1)} %all-gather.16.cloned.1.call-done, bf16[256,512]{1,0:T(8,128)(2,1)S(1)} %copy-done.2), kind=kOutput, calls=%fused_computation.49 | convolution fusion | flops 269483776 | bytes 2624512 | tf_op jit(solution)/shard_map/dot_general | solution.py:119
  166.5 5.6 %psum.15 = f32[256]{0:T(256)S(1)} all-reduce(f32[256]{0:T(256)S(1)} %get-tuple-element.267), channel_id=1, replica_groups=mesh['grp'=2,'sp'=4,'tp'=4] {'tp'}, use_global_device_ids=true, to_apply=%region_5.6 | all-reduce | flops 256 | bytes 2048 | tf_op jit(solution)/shard_map/psum | solution.py:70
  172.1 11.6 %all-gather.18.cloned.1.call-done = bf16[256,2048]{1,0:T(8,128)(2,1)} async-done(((bf16[256,512]{1,0:T(8,128)(2,1)}), bf16[256,2048]{1,0:T(8,128)(2,1)}) %all-gather.18.cloned.1.call-update) | async-done | bytes 1048592 | tf_op jit(solution)/shard_map/all_gather | solution.py:75
  183.7 2.0 fusion.20
  185.7 1.4 collective-permute-start.1
  187.4 2.8 %collective-permute-done.1 = bf16[256,3]{0,1:T(4,128)(2,1)S(1)} collective-permute-done((bf16[256,3]{0,1:T(4,128)(2,1)S(1)}, bf16[256,3]{0,1:T(4,128)(2,1)S(1)}, u32[]{:S(2)}, u32[]{:S(2)}) %collective-permute-start.1) | collective-permute-done | bytes 1568 | tf_op jit(solution)/shard_map/ppermute | solution.py:16
  190.2 0.1 fusion.85
  190.4 0.3 fusion.25
  190.7 0.3 fusion.28
  191.3 0.2 multiply_multiply_fusion
  191.5 0.2 slice.772
  191.9 0.2 slice.715
  194.7 5.6 %all-gather.2 = f32[1024,1]{0,1:T(1,128)S(1)} all-gather(f32[256,1]{0,1:T(1,128)S(1)} %slice_add_fusion.1), channel_id=4, replica_groups=mesh['grp'=2,'sp'=4,'tp'=4] {'sp'}, dimensions={0}, use_global_device_ids=true | all-gather | bytes 5120 | tf_op jit(solution)/shard_map/all_gather | solution.py:21
  200.3 0.6 reduce.14
  201.0 7.5 %all-gather.3 = f32[1024,1]{0,1:T(1,128)S(1)} all-gather(f32[256,1]{0,1:T(1,128)S(1)} %slice_add_fusion), channel_id=5, replica_groups=mesh['grp'=2,'sp'=4,'tp'=4] {'sp'}, dimensions={0}, use_global_device_ids=true | all-gather | bytes 5120 | tf_op jit(solution)/shard_map/all_gather | solution.py:21
  208.5 0.6 reduce.15
  209.2 0.2 while.29
  209.5 12.5 %all_gather.43 = bf16[1024,256]{0,1:T(8,128)(2,1)S(1)} all-gather(bf16[256,256]{0,1:T(8,128)(2,1)S(1)} %fusion.45), channel_id=1, replica_groups=mesh['grp'=2,'sp'=4,'tp'=4] {'tp'}, dimensions={0}, use_global_device_ids=true | all-gather | bytes 655360 | tf_op jit(solution)/shard_map/all_gather | solution.py:120
  221.9 2.4 %fusion.15 = bf16[256,512]{1,0:T(8,128)(2,1)} fusion(f32[256,512]{1,0:T(8,128)S(1)} %copy-done.9, bf16[1024,256]{0,1:T(8,128)(2,1)S(1)} %all_gather.43, bf16[2,1024,512]{2,1,0:T(8,128)(2,1)} %all-gather.16.cloned.1.call-done), kind=kOutput, calls=%fused_computation.19 | convolution fusion | flops 268697600 | bytes 2359296 | tf_op jit(solution)/shard_map/dot_general | solution.py:119
  (311 shorter events, 5.8 us)
Async XLA Ops:
  6.5 10.5 %copy-start.3 = (f32[2,4,256]{2,1,0:T(4,128)S(1)}, f32[2,4,256]{2,1,0:T(4,128)}, u32[]{:S(2)}) copy-start(f32[2,4,256]{2,1,0:T(4,128)} %param.18) | copy-start | bytes 24580
  6.5 10.5 %copy-start.1 = (f32[2,256,256]{2,1,0:T(8,128)S(1)}, f32[2,256,256]{2,1,0:T(8,128)}, u32[]{:S(2)}) copy-start(f32[2,256,256]{2,1,0:T(8,128)} %param.22) | copy-start | bytes 1572868
  6.5 10.6 %copy-start.4 = (f32[2,256]{1,0:T(2,128)S(1)}, f32[2,256]{1,0:T(2,128)}, u32[]{:S(2)}) copy-start(f32[2,256]{1,0:T(2,128)} %param.21) | copy-start | bytes 6148
  6.5 47.0 %all-gather.12.cloned.1.call-start = ((), (), s32[]{:S(2)}) async-start(), calls=%async_computation.1 | async-start | bytes 2621440 | tf_op jit(solution)/shard_map/all_gather | solution.py:59
  7.3 92.3 %all-gather.10.cloned.1.call-start = ((), (), s32[]{:S(2)}) async-start(), calls=%async_computation | async-start | bytes 2621440 | tf_op jit(solution)/shard_map/all_gather | solution.py:58
  8.0 110.2 %all-gather.14.cloned.1.call-start = ((), (), s32[]{:S(2)}) async-start(), calls=%async_computation.2 | async-start | bytes 1310720 | tf_op jit(solution)/shard_map/all_gather | solution.py:75
  10.7 153.3 %all-gather.16.cloned.1.call-start = ((), (), s32[]{:S(2)}) async-start(), calls=%async_computation.3 | async-start | bytes 2621440 | tf_op jit(solution)/shard_map/all_gather | solution.py:60
  11.2 172.5 %all-gather.18.cloned.1.call-start = ((), (), s32[]{:S(2)}) async-start(), calls=%async_computation.4 | async-start | bytes 1310720 | tf_op jit(solution)/shard_map/all_gather | solution.py:75
  118.2 7.1 %copy-start.5 = (bf16[2,4,64,64]{3,2,1,0:T(8,128)(2,1)S(1)}, bf16[2,4,64,64]{3,2,1,0:T(8,128)(2,1)}, u32[]{:S(2)}) copy-start(bf16[2,4,64,64]{3,2,1,0:T(8,128)(2,1)} %param.20) | copy-start | bytes 196612
  120.5 5.2 %copy-start.7 = (bf16[2,4,64,64]{3,2,1,0:T(8,128)(2,1)S(1)}, bf16[2,4,64,64]{3,2,1,0:T(8,128)(2,1)}, u32[]{:S(2)}) copy-start(bf16[2,4,64,64]{3,2,1,0:T(8,128)(2,1)} %param.19) | copy-start | bytes 196612
  120.5 4.5 %collective-permute-start = (bf16[256,3]{0,1:T(4,128)(2,1)S(1)}, bf16[256,3]{0,1:T(4,128)(2,1)S(1)}, u32[]{:S(2)}, u32[]{:S(2)}) collective-permute-start(bf16[256,3]{0,1:T(4,128)(2,1)S(1)} %slice.794), channel_id=1, source_target_pairs={{0,4},{4,8},{8,12},{1,5},{5,9},{9,13},{2,6},{6,10},{10,14},{3,7},{... | collective-permute-start | bytes 4616 | tf_op jit(solution)/shard_map/ppermute | solution.py:16
  129.3 34.7 %copy-start.2 = (bf16[256,512]{1,0:T(8,128)(2,1)S(1)}, bf16[256,512]{1,0:T(8,128)(2,1)}, u32[]{:S(2)}) copy-start(bf16[256,512]{1,0:T(8,128)(2,1)} %param.14) | copy-start | bytes 786436
  146.1 37.6 %copy-start = (bf16[256,2048]{1,0:T(8,128)(2,1)S(1)}, bf16[256,2048]{1,0:T(8,128)(2,1)}, u32[]{:S(2)}) copy-start(bf16[256,2048]{1,0:T(8,128)(2,1)} %get-tuple-element.259) | copy-start | bytes 3145732
  183.7 6.7 %copy-start.6 = (bf16[2,4,64,64]{3,2,1,0:T(8,128)(2,1)S(1)}, bf16[2,4,64,64]{3,2,1,0:T(8,128)(2,1)}, u32[]{:S(2)}) copy-start(bf16[2,4,64,64]{3,2,1,0:T(8,128)(2,1)} %param.20) | copy-start | bytes 196612
  185.7 5.0 %copy-start.8 = (bf16[2,4,64,64]{3,2,1,0:T(8,128)(2,1)S(1)}, bf16[2,4,64,64]{3,2,1,0:T(8,128)(2,1)}, u32[]{:S(2)}) copy-start(bf16[2,4,64,64]{3,2,1,0:T(8,128)(2,1)} %param.19) | copy-start | bytes 196612
  185.7 4.5 %collective-permute-start.1 = (bf16[256,3]{0,1:T(4,128)(2,1)S(1)}, bf16[256,3]{0,1:T(4,128)(2,1)S(1)}, u32[]{:S(2)}, u32[]{:S(2)}) collective-permute-start(bf16[256,3]{0,1:T(4,128)(2,1)S(1)} %slice.856), channel_id=1, source_target_pairs={{0,4},{4,8},{8,12},{1,5},{5,9},{9,13},{2,6},{6,10},{10,14},{3,7},{... | collective-permute-start | bytes 4616 | tf_op jit(solution)/shard_map/ppermute | solution.py:16
  194.5 27.5 %copy-start.9 = (f32[256,512]{1,0:T(8,128)S(1)}, f32[256,512]{1,0:T(8,128)}, u32[]{:S(2)}) copy-start(f32[256,512]{1,0:T(8,128)} %get-tuple-element.353) | copy-start | bytes 1572868
Sparse Core Ops, SparseCore 0:
  8.9 44.5 all-gather.11
  55.1 44.4 all-gather.9
  101.1 17.0 all-gather.13
  119.6 44.2 all-gather.15
  166.6 17.0 all-gather.17
where the time goes:
time: 234 us; the launch traced here: 231 us
  waiting for transfers between devices  121 us (52%)
  blocking collectives  63.4 us (27%)
  between operations  14.9 us (6%)
  local copies, waits for them, and re-layouts  11.5 us (5%)
  matrix products  10.3 us (4%)
  other arithmetic  6.39 us (3%)
  starting transfers between devices  3.01 us (1%)
    all_gather x1, waiting for transfers between devices, local(): lax.all_gather(value_proj, 'sp', axis=2, tiled=True)  44.4 us
    all_gather x1, waiting for transfers between devices, local(): lax.all_gather(gate_proj, 'sp', axis=2, tiled=True)  36.4 us
    all_gather x4, blocking collectives, carried_in(): pieces = jax.tree.map(lambda part: lax.all_gather(part, axis), value)  27.5 us
    all_gather x2, waiting for transfers between devices, local(): lax.all_gather(scaled, 'tp', axis=1, tiled=True)  27.1 us
    all_gather x2, blocking collectives, local(): lax.all_gather(branch, 'tp', axis=0, tiled=True)  24.6 us
    psum x2, blocking collectives, local(): squares = lax.psum(jnp.sum(wide * wide, axis=1), 'tp')  11.3 us
    all_gather x1, waiting for transfers between devices, local(): lax.all_gather(mix_proj, 'sp', axis=1, tiled=True)  5.71 us
    ppermute x2, waiting for transfers between devices, from_behind(): lax.ppermute(value, axis, [(source, source + steps) for source in range(f...  5.69 us
  transfers between devices with their start and end apart: 7, of which 7 were waited for; matrix products, arithmetic and copies ran while one was open for 7% of the time, Pallas kernels for 0%

commit v1 on v0

v1 whole, which is shorter than its diff:
```python
import functools
import math

import jax
import jax.numpy as jnp
from jax import lax
from jax.experimental import pallas as pl
from jax.experimental.pallas import tpu as pltpu
from jax.sharding import PartitionSpec as P

EPS = 1e-06
RATE_SCALE = 8.0
HALO = 16
MESH = pl.DeviceIdType.MESH
NT = (((1,), (1,)), ((), ()))


def softplus(v):
    u = jnp.exp(-jnp.abs(v))
    series = jnp.full_like(u, 1.0 / 9.0)
    for term in range(8, 0, -1):
        series = 1.0 / term - u * series
    return jnp.maximum(v, 0.0) + jnp.where(u < 0.1, u * series, jnp.log(1.0 + u))


def one_minus_exp(y, exp_y):
    series = jnp.full_like(y, 1.0)
    for term in range(8, 1, -1):
        series = 1.0 + y * series * (1.0 / term)
    return jnp.where(y > -0.5, -y * series, 1.0 - exp_y)


def sigmoid(v):
    return 1.0 / (1.0 + jnp.exp(-v))


def kernel(
    groups, sp_count, tp_count, layers,
    tokens, gains, value, gate, taps_ref, recur, inmap, param, offset, mix, out,
    vbuf, gbuf, mbuf, scbuf, ssbuf, brbuf, halo_out, halo_in, end_out, end_in, carry, blocks, offs, wide,
    zsend, zrecv, ysend, yrecv, gsend, grecv, fsend, ssend, srecv, sfsend, bsend, brecv, bfsend,
    hsend, hrecv, csend, crecv,
):
    grp, me, tp = lax.axis_index("grp"), lax.axis_index("sp"), lax.axis_index("tp")
    rows, own_cols = tokens.shape
    channels = value.shape[1]
    head = recur.shape[2]
    heads = recur.shape[1]
    tap_total = taps_ref.shape[1]
    paired = tp_count % 2 == 0
    partner = tp + 1 - 2 * lax.rem(tp, 2)

    same = [lax.rem(tp + 2 * k, tp_count) for k in range(1, tp_count // 2)] if paired else [
        lax.rem(tp + k, tp_count) for k in range(1, tp_count)]
    same_from = [lax.rem(tp + tp_count - 2 * k, tp_count) for k in range(1, tp_count // 2)] if paired else [
        lax.rem(tp + tp_count - k, tp_count) for k in range(1, tp_count)]
    other_groups = [lax.rem(grp + k, groups) for k in range(1, groups)]
    group_from = [lax.rem(grp + groups - k, groups) for k in range(1, groups)]

    barrier = pltpu.get_barrier_semaphore()
    greeted = 0
    for peer in same + ([partner] if paired else []):
        pl.semaphore_signal(barrier, inc=1, device_id={"tp": peer}, device_id_type=MESH)
        greeted += 1
    for k in range(1, sp_count):
        pl.semaphore_signal(barrier, inc=1, device_id={"sp": lax.rem(me + k, sp_count)}, device_id_type=MESH)
        greeted += 1
    for peer in other_groups:
        pl.semaphore_signal(barrier, inc=1, device_id={"grp": peer}, device_id_type=MESH)
        greeted += 1
    pl.semaphore_wait(barrier, greeted)

    def remote(src, dst, send, recv, axis, peer):
        return pltpu.make_async_remote_copy(
            src_ref=src, dst_ref=dst, send_sem=send, recv_sem=recv, device_id={axis: peer}, device_id_type=MESH)

    class Gather:
        def __init__(self, buf, layer, cuts, sems):
            self.buf, self.layer, self.sems = buf, layer, sems
            size = buf.shape[2] // cuts
            self.views = [pl.ds(c * size, size) for c in range(cuts)]

        def copy(self, cut, slot, sem, number, peer):
            part = self.buf.at[self.layer, slot, self.views[cut]]
            return remote(part, part, sem.at[self.layer, cut, number], self.sems[1].at[self.layer, cut, slot], "tp", peer)

        def start(self):
            for cut in range(len(self.views)):
                for number, peer in enumerate(same):
                    self.copy(cut, tp, self.sems[0], number, peer).start()
                if paired:
                    self.copy(cut, tp, self.sems[0], len(same), partner).start()

        def finish(self):
            for cut in range(len(self.views)):
                for number, source in enumerate(same_from):
                    self.copy(cut, source, self.sems[0], number, partner).wait_recv()
                    if paired:
                        self.copy(cut, source, self.sems[2], number, partner).start()
            if paired:
                for cut in range(len(self.views)):
                    self.copy(cut, partner, self.sems[0], 0, partner).wait_recv()
                    for number in range(len(same)):
                        source = lax.rem(partner + tp_count - 2 * (number + 1), tp_count)
                        self.copy(cut, source, self.sems[0], number, partner).wait_recv()

        def drain(self):
            for cut in range(len(self.views)):
                for number in range(len(same) + (1 if paired else 0)):
                    self.copy(cut, tp, self.sems[0], number, partner).wait_send()
                if paired:
                    for number, source in enumerate(same_from):
                        self.copy(cut, source, self.sems[2], number, partner).wait_send()

    parts = []
    for layer in range(layers):
        parts += [(value, vbuf, layer), (gate, gbuf, layer), (mix, mbuf, layer)]

    def share(number):
        size = parts[number][0].shape[1] // groups
        return pl.ds(pl.multiple_of(grp * size, size), size)

    def z_copy(number, way, step):
        own, buf, layer = parts[number]
        source = me - way * (step - 1)
        src = own.at[layer, share(number)] if step == 1 else buf.at[layer, source, share(number)]
        valid = (source >= 0) & (source < sp_count) & (me + way >= 0) & (me + way < sp_count)
        slot = jnp.clip(source, 0, sp_count - 1)
        if step > 1:
            src = buf.at[layer, slot, share(number)]
        copy = remote(src, buf.at[layer, slot, share(number)], zsend.at[number, (way + 1) // 2, step - 1],
                      zrecv.at[number, slot], "sp", jnp.clip(me + way, 0, sp_count - 1))
        return valid, copy

    def y_copy(number, source, which, peer):
        _, buf, layer = parts[number]
        part = buf.at[layer, source, share(number)]
        return remote(part, part, ysend.at[number, source, which], yrecv.at[number, source, which], "grp", peer)

    def own_send(number):
        for way in (1, -1):
            valid, copy = z_copy(number, way, 1)
            pl.when(valid)(copy.start)

    def pump(number, third):
        per = -(-(sp_count - 1) // 3)
        for step in range(third * per + 1, min((third + 1) * per, sp_count - 1) + 1):
            for way in (1, -1):
                source = me - way * step
                valid = (source >= 0) & (source < sp_count)
                slot = jnp.clip(source, 0, sp_count - 1)
                _, buf, layer = parts[number]

                @pl.when(valid)
                def _():
                    part = buf.at[layer, slot, share(number)]
                    remote(part, part, zsend.at[number, 0, 0], zrecv.at[number, slot], "sp",
                           lax.rem(me + 1, sp_count)).wait_recv()
                    for which, peer in enumerate(other_groups):
                        y_copy(number, slot, which, peer).start()

                if step < sp_count - 1:
                    going, copy = z_copy(number, way, step + 1)
                    pl.when(going)(copy.start)

    def y_wait(number):
        _, buf, layer = parts[number]
        size = parts[number][0].shape[1] // groups
        for k in range(1, sp_count):
            source = lax.rem(me + k, sp_count)
            for which, peer in enumerate(group_from):
                part = buf.at[layer, source, pl.ds(pl.multiple_of(peer * size, size), size)]
                remote(part, part, ysend.at[number, source, which], yrecv.at[number, source, which],
                       "grp", other_groups[0]).wait_recv()

    gathers = []

    def normed(layer):
        x = wide[...]
        own_gain = gains[layer, :, pl.ds(pl.multiple_of(tp * own_cols, own_cols), own_cols)]
        scbuf[layer, tp] = (x * own_gain).astype(jnp.bfloat16)
        ssbuf[layer, tp] = lax.dot_general(
            jnp.ones((8, own_cols), jnp.float32), x * x, NT,
            precision=lax.Precision.HIGHEST, preferred_element_type=jnp.float32)
        small = Gather(ssbuf, layer, 1, (ssend, srecv, sfsend))
        large = Gather(scbuf, layer, 2, (gsend, grecv, fsend))
        gathers.extend([small, large])
        small.start()
        large.start()
        return small, large

    def project(layer, buf):
        cols = buf.shape[3]
        chunk = math.gcd(cols, own_cols)
        total = None
        for at in range(0, cols * sp_count, chunk):
            left = scbuf[layer, at // own_cols, :, at % own_cols : at % own_cols + chunk]
            right = buf[layer, at // cols, :, at % cols : at % cols + chunk]
            term = lax.dot_general(left, right, NT, preferred_element_type=jnp.float32)
            total = term if total is None else total + term
        return total

    wide[...] = tokens[...].astype(jnp.float32)
    pending = normed(0)
    for number in range(3):
        own_send(number)
    for layer in range(layers):
        vbuf[layer, me] = value[layer]
        gbuf[layer, me] = gate[layer]
        mbuf[layer, me] = mix[layer]
        offs[layer] = offset[layer].T
        for kind, source in enumerate((recur, inmap)):
            blocks[layer, kind] = jnp.zeros((channels, channels), jnp.bfloat16)
            for number in range(heads):
                cut = slice(number * head, (number + 1) * head)
                blocks[layer, kind, cut, cut] = source[layer, number]

    for layer in range(layers):
        first = 3 * layer
        more = layer + 1 < layers
        if layer == 0:
            for number in (first, first + 1):
                pump(number, 0)
            if more:
                own_send(first + 3)
                own_send(first + 4)
            for number in (first, first + 1):
                pump(number, 1)
            pump(first + 2, 0)
        for gather in pending:
            gather.finish()
        for number in (first, first + 1):
            pump(number, 2)
        if layer > 0:
            pump(first + 2, 0)
        y_wait(first)
        y_wait(first + 1)
        squares = ssbuf[layer, 0]
        for source in range(1, tp_count):
            squares = squares + ssbuf[layer, source]
        scale = lax.rsqrt(squares / (own_cols * tp_count) + EPS).T[:, 0:1]
        value_half = (project(layer, vbuf) * scale).astype(jnp.bfloat16)
        halo_out[layer] = value_half[rows - HALO :]
        halo_copy = remote(halo_out.at[layer], halo_in.at[layer], hsend.at[layer], hrecv.at[layer], "sp",
                           jnp.minimum(me + 1, sp_count - 1))
        pl.when(me < sp_count - 1)(halo_copy.start)
        gate_rows = (project(layer, gbuf) * scale).astype(jnp.bfloat16).astype(jnp.float32)
        silu = gate_rows / (1.0 + jnp.exp(-gate_rows))
        pump(first + 2, 1)
        if more:
            own_send(first + 5)

        @pl.when(me == 0)
        def _():
            halo_in[layer] = jnp.zeros((HALO, channels), jnp.bfloat16)

        pl.when(me > 0)(halo_copy.wait_recv)
        longer = jnp.concatenate(
            [halo_in[layer].astype(jnp.float32), value_half.astype(jnp.float32)], axis=0)
        smoothed = jnp.zeros((rows, channels), jnp.float32)
        for tap in range(tap_total):
            behind = tap_total - 1 - tap
            shifted = pltpu.roll(longer, behind, 0) if behind else longer
            smoothed = smoothed + taps_ref[layer, tap : tap + 1, :] * shifted[HALO:]
        half = smoothed.astype(jnp.bfloat16)
        recur_gate = sigmoid(jnp.dot(half, blocks[layer, 0], preferred_element_type=jnp.float32))
        input_gate = sigmoid(jnp.dot(half, blocks[layer, 1], preferred_element_type=jnp.float32))
        rate = -RATE_SCALE * softplus(-param[layer])
        log_decay = recur_gate * rate + offs[layer]
        a = jnp.exp(log_decay)
        b = jnp.sqrt(one_minus_exp(2.0 * log_decay, a * a)) * input_gate * smoothed
        index = lax.broadcasted_iota(jnp.int32, (rows, channels), 0)
        reach = 1
        while reach < rows:
            inside = index >= reach
            b = b + a * jnp.where(inside, pltpu.roll(b, reach, 0), 0.0)
            a = a * jnp.where(inside, pltpu.roll(a, reach, 0), 1.0)
            reach *= 2
        end_out[layer, 0:8] = a[rows - 8 :]
        end_out[layer, 8:16] = b[rows - 8 :]
        for k in range(1, sp_count):
            peer = jnp.minimum(me + k, sp_count - 1)
            pl.when(me + k < sp_count)(
                remote(end_out.at[layer], end_in.at[layer, me], csend.at[layer, k - 1], crecv.at[layer, me],
                       "sp", peer).start)
        pump(first + 2, 2)
        if more:
            pump(first + 3, 0)
            pump(first + 4, 0)
        carry[...] = jnp.zeros((8, channels), jnp.float32)
        for source in range(sp_count - 1):

            @pl.when(source < me)
            def _():
                remote(end_out.at[layer], end_in.at[layer, source], csend.at[layer, 0], crecv.at[layer, source],
                       "sp", lax.rem(me + 1, sp_count)).wait_recv()
                carry[...] = end_in[layer, source, 0:8] * carry[...] + end_in[layer, source, 8:16]
                carry[...] = jnp.broadcast_to(carry[7:8], (8, channels))

        brbuf[layer, tp] = ((b + a * carry[0:1]) * silu).astype(jnp.bfloat16)
        branches = Gather(brbuf, layer, 1, (bsend, brecv, bfsend))
        gathers.append(branches)
        branches.start()
        if more:
            pump(first + 3, 1)
            pump(first + 4, 1)
        y_wait(first + 2)
        branches.finish()
        chunk_rows = mbuf.shape[2]
        chunk = math.gcd(chunk_rows, channels)
        total = wide[...]
        for at in range(0, channels * tp_count, chunk):
            total = total + jnp.dot(
                brbuf[layer, at // channels, :, at % channels : at % channels + chunk],
                mbuf[layer, at // chunk_rows, at % chunk_rows : at % chunk_rows + chunk, :],
                preferred_element_type=jnp.float32)
        rounded = total.astype(jnp.bfloat16)
        if more:
            wide[...] = rounded.astype(jnp.float32)
            pending = normed(layer + 1)
        else:
            out[...] = rounded

    for gather in gathers:
        gather.drain()
    for number in range(len(parts)):
        for step in range(1, sp_count):
            for way in (1, -1):
                valid, copy = z_copy(number, way, step)
                pl.when(valid)(copy.wait_send)
            source = lax.rem(me + step, sp_count)
            for which, peer in enumerate(other_groups):
                y_copy(number, source, which, peer).wait_send()
    for layer in range(layers):
        pl.when(me < sp_count - 1)(
            remote(halo_out.at[layer], halo_in.at[layer], hsend.at[layer], hrecv.at[layer], "sp",
                   jnp.minimum(me + 1, sp_count - 1)).wait_send)
        for k in range(1, sp_count):
            pl.when(me + k < sp_count)(
                remote(end_out.at[layer], end_in.at[layer, me], csend.at[layer, k - 1], crecv.at[layer, me],
                       "sp", jnp.minimum(me + k, sp_count - 1)).wait_send)


def local(sizes, tokens, norm_gain, value_proj, gate_proj, conv_taps, recur_map, input_map, decay_param,
          decay_offset, mix_proj):
    groups, sp_count, tp_count = sizes
    layers = value_proj.shape[0]
    rows, own_cols = tokens.shape
    channels = value_proj.shape[1]
    bf, f32 = jnp.bfloat16, jnp.float32
    same = tp_count // 2
    dma = pltpu.SemaphoreType.DMA
    count = 3 * layers
    peers = max(groups - 1, 1)
    direct, fwd = tp_count, max(same, 1)
    scratch = [
        pltpu.VMEM((layers, sp_count) + value_proj.shape[1:], bf),
        pltpu.VMEM((layers, sp_count) + gate_proj.shape[1:], bf),
        pltpu.VMEM((layers, sp_count) + mix_proj.shape[1:], bf),
        pltpu.VMEM((layers, tp_count, rows, own_cols), bf),
        pltpu.VMEM((layers, tp_count, 8, rows), f32),
        pltpu.VMEM((layers, tp_count, rows, channels), bf),
        pltpu.VMEM((layers, HALO, channels), bf),
        pltpu.VMEM((layers, HALO, channels), bf),
        pltpu.VMEM((layers, 16, channels), f32),
        pltpu.VMEM((layers, sp_count, 16, channels), f32),
        pltpu.VMEM((8, channels), f32),
        pltpu.VMEM((layers, 2, channels, channels), bf),
        pltpu.VMEM((layers, rows, channels), f32),
        pltpu.VMEM((rows, own_cols), f32),
        dma((count, 2, sp_count)), dma((count, sp_count)), dma((count, sp_count, peers)), dma((count, sp_count, peers)),
        dma((layers, 2, direct)), dma((layers, 2, tp_count)), dma((layers, 2, fwd)),
        dma((layers, 1, direct)), dma((layers, 1, tp_count)), dma((layers, 1, fwd)),
        dma((layers, 1, direct)), dma((layers, 1, tp_count)), dma((layers, 1, fwd)),
        dma((layers,)), dma((layers,)), dma((layers, sp_count)), dma((layers, sp_count)),
    ]
    vmem = pl.BlockSpec(memory_space=pltpu.VMEM)
    return pl.pallas_call(
        functools.partial(kernel, groups, sp_count, tp_count, layers),
        out_shape=jax.ShapeDtypeStruct((rows, own_cols), bf),
        in_specs=[vmem] * 10,
        out_specs=vmem,
        scratch_shapes=scratch,
        compiler_params=pltpu.CompilerParams(
            collective_id=0, has_side_effects=True, vmem_limit_bytes=60 * 1024 * 1024),
    )(tokens, norm_gain[:, None, :], value_proj, gate_proj, conv_taps, recur_map, input_map,
      decay_param[:, None, :], decay_offset, mix_proj)


def solution(mesh):
    in_specs = (
        P(("grp", "sp"), "tp"),
        P(),
        P(None, "tp", "sp"),
        P(None, "tp", "sp"),
        P(None, None, "tp"),
        P(None, "tp", None, None),
        P(None, "tp", None, None),
        P(None, "tp"),
        P(None, "tp", "sp"),
        P(None, "sp", "tp"),
    )
    out_specs = P(("grp", "sp"), "tp")
    sizes = (mesh.shape["grp"], mesh.shape["sp"], mesh.shape["tp"])
    return jax.shard_map(
        functools.partial(local, sizes), mesh=mesh, in_specs=in_specs, out_specs=out_specs, check_vma=False)
```

time: 234 us -> 88.8 us (0.38); the launches traced: 231 us -> 88.5 us
  waiting for transfers between devices: 121 us -> 0 us
  Pallas kernels: 0 us -> 84.3 us
  blocking collectives: 63.4 us -> 0 us
  between operations: 14.9 us -> 0.01 us
  matrix products: 10.3 us -> 0 us
  local copies, waits for them, and re-layouts: 11.5 us -> 4.26 us
  other arithmetic: 6.39 us -> 0 us
  starting transfers between devices: 3.01 us -> 0 us
    all_gather x5 -> x0, waiting for transfers between devices: 114 us -> none  [the longest x1 44.4 us: local(): lax.all_gather(value_proj, 'sp', axis=2, tiled=True)]
    pallas_call x0 -> x1, Pallas kernels: none -> 84.3 us  [local(): pl.pallas_call(functools.partial(kernel, groups, sp_count, tp_count, laye...]
    all_gather x6 -> x0, blocking collectives: 52.1 us -> none  [the longest x4 27.5 us: carried_in(): pieces = jax.tree.map(lambda part: lax.all_gather(part, axis), value)]
    psum x2 -> x0, blocking collectives: 11.3 us -> none  [local(): squares = lax.psum(jnp.sum(wide * wide, axis=1), 'tp')]
    dot_general x8 -> x0, matrix products: 10.3 us -> none  [the longest x2 4.93 us: local(): lax.dot_general(lax.all_gather(branch, 'tp', axis=0, tiled=True), mix_wei...]
    ppermute x2 -> x0, waiting for transfers between devices: 5.69 us -> none  [from_behind(): lax.ppermute(value, axis, [(source, source + steps) for source in range(f...]
    squeeze x2 -> x0, local copies, waits for them, and re-layouts: 4.83 us -> none  [the longest x1 3.16 us: local(): value_weights = every_value[layer_index]]
    slice x111 -> x0, local copies, waits for them, and re-layouts: 4.1 us -> none  [the longest x104 3.21 us: local(): lax.associative_scan(combine_pairs, (decay, driving), axis=1)]
  transfers between devices with their start and end apart: 7 -> 0, of which waited for: 7 -> 0; matrix products, arithmetic and copies ran while one was open for 7% -> 0% of each run, Pallas kernels for 0% -> 0%
where the time goes in v1:
time: 88.8 us; the launch traced here: 88.5 us
  Pallas kernels  84.3 us (95%)
  local copies, waits for them, and re-layouts  4.26 us (5%)
    pallas_call x1, Pallas kernels, local(): pl.pallas_call(functools.partial(kernel, groups, sp_count, tp_count, laye...  84.3 us

profile of v1, /device:TPU:27, one launch (start us, length us, event | category | flops | bytes accessed | tf_op | source)
XLA Modules:
  0.0 88.5 jit_solution(4745805385335657227)
XLA Ops:
  0.0 1.3 %broadcast_in_dim.7.param = f32[2,1,256]{2,1,0:T(1,128)} reshape(f32[2,256]{1,0:T(2,128)} %param.17) | data formatting | bytes 4096 | tf_op jit(solution)/shard_map/broadcast_in_dim | solution.py:387
  1.3 1.3 %broadcast_in_dim.6.gains = f32[2,1,2048]{2,1,0:T(1,128)} reshape(f32[2,2048]{1,0:T(2,128)} %param.11) | data formatting | bytes 32768 | tf_op jit(solution)/shard_map/broadcast_in_dim | solution.py:386
  2.6 84.3 %shard_map.100 = bf16[256,512]{1,0:T(8,128)(2,1)} custom-call(bf16[256,512]{1,0:T(8,128)(2,1)} %tokens.1, f32[2,1,2048]{2,1,0:T(1,128)} %broadcast_in_dim.6.gains, bf16[2,256,512]{2,1,0:T(8,128)(2,1)} %value.1, bf16[2,256,512]{2,1,0:T(8,128)(2,1)} %gate.1, f32[2,4,256]{2,1,0:T(4,128)} %taps_ref.1, bf16[2,4,64,64]{3,2,1,0:T(8,128)(2,1)} %recur.1, ...), custom_call_target="tpu_custom_call" | custom-call | tf_op jit(solution)/shard_map/pallas_call | solution.py:378
  86.9 1.7 %copy.12 = bf16[256,512]{1,0:T(8,128)(2,1)} copy(bf16[256,512]{1,0:T(8,128)(2,1)} %shard_map.100) | data formatting | bytes 524288

commit v2 on v1

--- a/solution.py
+++ b/solution.py
@@ -11,6 +11,7 @@
 EPS = 1e-06
 RATE_SCALE = 8.0
 HALO = 16
+PIECES = 1
 MESH = pl.DeviceIdType.MESH
 NT = (((1,), (1,)), ((), ()))
 
@@ -114,11 +115,12 @@
 
     parts = []
     for layer in range(layers):
-        parts += [(value, vbuf, layer), (gate, gbuf, layer), (mix, mbuf, layer)]
-
-    def share(number):
-        size = parts[number][0].shape[1] // groups
-        return pl.ds(pl.multiple_of(grp * size, size), size)
+        for own, buf in ((value, vbuf), (gate, gbuf), (mix, mbuf)):
+            parts += [(own, buf, layer)] * PIECES
+
+    def share(number, carrier=grp):
+        size = parts[number][0].shape[1] // (groups * PIECES)
+        return pl.ds(pl.multiple_of((number % PIECES * groups + carrier) * size, size), size)
 
     def z_copy(number, way, step):
         own, buf, layer = parts[number]
@@ -137,41 +139,49 @@
         part = buf.at[layer, source, share(number)]
         return remote(part, part, ysend.at[number, source, which], yrecv.at[number, source, which], "grp", peer)
 
-    def own_send(number):
-        for way in (1, -1):
-            valid, copy = z_copy(number, way, 1)
-            pl.when(valid)(copy.start)
-
-    def pump(number, third):
+    def own_send(base):
+        for number in range(base * PIECES, (base + 1) * PIECES):
+            for way in (1, -1):
+                valid, copy = z_copy(number, way, 1)
+                pl.when(valid)(copy.start)
+
+    def pump(base, third):
         per = -(-(sp_count - 1) // 3)
         for step in range(third * per + 1, min((third + 1) * per, sp_count - 1) + 1):
-            for way in (1, -1):
-                source = me - way * step
-                valid = (source >= 0) & (source < sp_count)
-                slot = jnp.clip(source, 0, sp_count - 1)
-                _, buf, layer = parts[number]
-
-                @pl.when(valid)
-                def _():
-                    part = buf.at[layer, slot, share(number)]
-                    remote(part, part, zsend.at[number, 0, 0], zrecv.at[number, slot], "sp",
-                           lax.rem(me + 1, sp_count)).wait_recv()
-                    for which, peer in enumerate(other_groups):
-                        y_copy(number, slot, which, peer).start()
-
-                if step < sp_count - 1:
-                    going, copy = z_copy(number, way, step + 1)
-                    pl.when(going)(copy.start)
-
-    def y_wait(number):
+            for number in range(base * PIECES, (base + 1) * PIECES):
+                for way in (1, -1):
+                    pump_piece(number, step, way)
+
+    def pump_piece(number, step, way):
+        source = me - way * step
+        valid = (source >= 0) & (source < sp_count)
+        slot = jnp.clip(source, 0, sp_count - 1)
         _, buf, layer = parts[number]
-        size = parts[number][0].shape[1] // groups
-        for k in range(1, sp_count):
-            source = lax.rem(me + k, sp_count)
-            for which, peer in enumerate(group_from):
-                part = buf.at[layer, source, pl.ds(pl.multiple_of(peer * size, size), size)]
-                remote(part, part, ysend.at[number, source, which], yrecv.at[number, source, which],
-                       "grp", other_groups[0]).wait_recv()
+
+        @pl.when(valid)
+        def _():
+            part = buf.at[layer, slot, share(number)]
+            remote(part, part, zsend.at[number, 0, 0], zrecv.at[number, slot], "sp",
+                   lax.rem(me + 1, sp_count)).wait_recv()
+
+        if step < sp_count - 1:
+            going, copy = z_copy(number, way, step + 1)
+            pl.when(going)(copy.start)
+
+        @pl.when(valid)
+        def _():
+            for which, peer in enumerate(other_groups):
+                y_copy(number, slot, which, peer).start()
+
+    def y_wait(base):
+        for number in range(base * PIECES, (base + 1) * PIECES):
+            _, buf, layer = parts[number]
+            for k in range(1, sp_count):
+                source = lax.rem(me + k, sp_count)
+                for which, peer in enumerate(group_from):
+                    part = buf.at[layer, source, share(number, peer)]
+                    remote(part, part, ysend.at[number, source, which], yrecv.at[number, source, which],
+                           "grp", other_groups[0]).wait_recv()
 
     gathers = []
 
@@ -200,10 +210,10 @@
             total = term if total is None else total + term
         return total
 
+    own_send(0)
+    own_send(1)
     wide[...] = tokens[...].astype(jnp.float32)
     pending = normed(0)
-    for number in range(3):
-        own_send(number)
     for layer in range(layers):
         vbuf[layer, me] = value[layer]
         gbuf[layer, me] = gate[layer]
@@ -219,20 +229,27 @@
         first = 3 * layer
         more = layer + 1 < layers
         if layer == 0:
-            for number in (first, first + 1):
-                pump(number, 0)
+            pump(first, 0)
+            pump(first + 1, 0)
+            own_send(first + 2)
+            for gather in pending:
+                gather.finish()
+            pump(first, 1)
+            pump(first + 1, 1)
             if more:
                 own_send(first + 3)
+            pump(first + 2, 0)
+            if more:
                 own_send(first + 4)
-            for number in (first, first + 1):
-                pump(number, 1)
+            pump(first, 2)
+            pump(first + 1, 2)
+            pump(first + 2, 1)
+        else:
             pump(first + 2, 0)
-        for gather in pending:
-            gather.finish()
-        for number in (first, first + 1):
-            pump(number, 2)
-        if layer > 0:
-            pump(first + 2, 0)
+            pump(first, 2)
+            for gather in pending:
+                gather.finish()
+            pump(first + 1, 2)
         y_wait(first)
         y_wait(first + 1)
         squares = ssbuf[layer, 0]
@@ -246,9 +263,11 @@
         pl.when(me < sp_count - 1)(halo_copy.start)
         gate_rows = (project(layer, gbuf) * scale).astype(jnp.bfloat16).astype(jnp.float32)
         silu = gate_rows / (1.0 + jnp.exp(-gate_rows))
-        pump(first + 2, 1)
         if more:
             own_send(first + 5)
+            pump(first + 3, 0)
+        if layer > 0:
+            pump(first + 2, 1)
 
         @pl.when(me == 0)
         def _():
@@ -285,7 +304,6 @@
                        "sp", peer).start)
         pump(first + 2, 2)
         if more:
-            pump(first + 3, 0)
             pump(first + 4, 0)
         carry[...] = jnp.zeros((8, channels), jnp.float32)
         for source in range(sp_count - 1):
@@ -350,7 +368,7 @@
     bf, f32 = jnp.bfloat16, jnp.float32
     same = tp_count // 2
     dma = pltpu.SemaphoreType.DMA
-    count = 3 * layers
+    count = 3 * layers * PIECES
     peers = max(groups - 1, 1)
     direct, fwd = tp_count, max(same, 1)
     scratch = [

time: 88.8 us -> 82.2 us (0.926)
  Pallas kernels: 84.3 us -> 77.7 us
    pallas_call x1, Pallas kernels: 84.3 us -> 77.7 us  [local(): pl.pallas_call(functools.partial(kernel, groups, sp_count, tp_count, laye...]
where the time goes in v2:
time: 82.2 us; the launch traced here: 81.9 us
  Pallas kernels  77.7 us (95%)
  local copies, waits for them, and re-layouts  4.26 us (5%)
    pallas_call x1, Pallas kernels, local(): pl.pallas_call(functools.partial(kernel, groups, sp_count, tp_count, laye...  77.7 us
    unnamed x1, local copies, waits for them, and re-layouts  1.67 us

profile of v2, /device:TPU:27, one launch (start us, length us, event | category | flops | bytes accessed | tf_op | source)
XLA Modules:
  0.0 81.9 jit_solution(10782652701186608723)
XLA Ops:
  0.0 1.3 %broadcast_in_dim.7.param = f32[2,1,256]{2,1,0:T(1,128)} reshape(f32[2,256]{1,0:T(2,128)} %param.17) | data formatting | bytes 4096 | tf_op jit(solution)/shard_map/broadcast_in_dim | solution.py:405
  1.3 1.3 %broadcast_in_dim.6.gains = f32[2,1,2048]{2,1,0:T(1,128)} reshape(f32[2,2048]{1,0:T(2,128)} %param.11) | data formatting | bytes 32768 | tf_op jit(solution)/shard_map/broadcast_in_dim | solution.py:404
  2.6 77.7 %shard_map.100 = bf16[256,512]{1,0:T(8,128)(2,1)} custom-call(bf16[256,512]{1,0:T(8,128)(2,1)} %tokens.1, f32[2,1,2048]{2,1,0:T(1,128)} %broadcast_in_dim.6.gains, bf16[2,256,512]{2,1,0:T(8,128)(2,1)} %value.1, bf16[2,256,512]{2,1,0:T(8,128)(2,1)} %gate.1, f32[2,4,256]{2,1,0:T(4,128)} %taps_ref.1, bf16[2,4,64,64]{3,2,1,0:T(8,128)(2,1)} %recur.1, ...), custom_call_target="tpu_custom_call" | custom-call | tf_op jit(solution)/shard_map/pallas_call | solution.py:396
  80.3 1.7 %copy.12 = bf16[256,512]{1,0:T(8,128)(2,1)} copy(bf16[256,512]{1,0:T(8,128)(2,1)} %shard_map.100) | data formatting | bytes 524288
